TPU v7x, 32 devices: a whole 2x2x4 slice. The times are simulated.
32 devices in a mesh: ep: 8 (over z, core), tp: 4 (over y, x).
Axes of the slice: x: 2, y: 2, z: 4, core: 2. Of those that a mesh axis runs over, the one named last changes fastest.
Arguments:
- tokens: bfloat16 [512, 4096], P('ep', 'tp'), may hold values from -600 to 600
- in_gain: float32 [4096], P('tp'), may hold values from 0.1 to 1.9
- out_gain: float32 [4096], P('tp'), may hold values from 0.1 to 1.9
- routes: int32 [512, 4], replicated, may hold values from 0 to 31, as said below
- route_weights: float32 [512, 4], replicated, may hold values from 0.05 to 1
- w_gate: bfloat16 [32, 4096, 1024], P('ep', 'tp'), may hold values from -0.09375 to 0.09375
- w_up: bfloat16 [32, 4096, 1024], P('ep', 'tp'), may hold values from -0.09375 to 0.09375
- w_down: bfloat16 [32, 1024, 4096], P('ep', None, 'tp'), may hold values from -0.375 to 0.375
Outputs:
- result: bfloat16 [512, 4096], P('ep', 'tp')
Inputs may be any that keep to these rules, and one draw needn't show every extreme that they name: `routes`: each row names 4 different experts, all in one group of 8 consecutive numbers. In the rows of one index of ep (aligned blocks of 64 rows) no expert is named by more than 16 rows, and some expert by exactly 16.
All inputs are finite; a program needn't handle non-finite values.
Results may differ from a plain program's by a relative error of at most 0.025.
Values may be sent and summed in bfloat16 or wider, within the bound.
A program may use at most 64 MiB of HBM per device.

v0:
```python
import jax
import jax.numpy as jnp
from jax import lax
from jax.sharding import PartitionSpec as P

D = 4096
EPS = 1e-06


def run_experts(slot_rows, w_gate, w_up, w_down):
    gate_part = jnp.einsum(
        "secd,edf->secf", slot_rows, w_gate, preferred_element_type=jnp.float32
    ).astype(jnp.bfloat16)
    up_part = jnp.einsum(
        "secd,edf->secf", slot_rows, w_up, preferred_element_type=jnp.float32
    ).astype(jnp.bfloat16)
    gate_sum, up_sum = (
        lax.psum(gate_part, "tp").astype(jnp.float32),
        lax.psum(up_part, "tp").astype(jnp.float32),
    )
    active = (jax.nn.silu(gate_sum) * up_sum).astype(jnp.bfloat16)
    return jnp.einsum("secf,efd->secd", active, w_down, preferred_element_type=jnp.float32).astype(
        jnp.bfloat16
    )


def on_device(tokens, in_gain, out_gain, routes, route_weights, w_gate, w_up, w_down):
    tok_rows, local_width = tokens.shape
    top_count = routes.shape[1]
    local_experts = w_gate.shape[0]
    groups_ep = lax.axis_size("ep")
    experts = local_experts * groups_ep
    capacity = max(2, 2 * tok_rows * top_count // experts)
    values = tokens.astype(jnp.float32)
    sum_squares = lax.psum(jnp.sum(values * values, axis=1), "tp")
    normed = (values * lax.rsqrt(sum_squares / D + EPS)[:, None] * in_gain).astype(jnp.bfloat16)
    row_start = lax.axis_index("ep") * tok_rows
    my_routes = lax.dynamic_slice_in_dim(routes, row_start, tok_rows, 0)
    my_weights = lax.dynamic_slice_in_dim(route_weights, row_start, tok_rows, 0)
    flat_ids = my_routes.reshape(-1)
    matches = (flat_ids[:, None] == jnp.arange(experts, dtype=jnp.int32)[None, :]).astype(jnp.int32)
    slot_rank = jnp.sum((jnp.cumsum(matches, axis=0) - matches) * matches, axis=1)
    position = flat_ids * capacity + slot_rank
    dispatch_table = jnp.any(
        position.reshape(tok_rows, top_count, 1)
        == jnp.arange(experts * capacity, dtype=jnp.int32)[None, None, :],
        axis=1,
    )
    outgoing = jnp.einsum(
        "ts,td->sd", dispatch_table.astype(jnp.bfloat16), normed, preferred_element_type=jnp.float32
    ).astype(jnp.bfloat16)
    outgoing = outgoing.reshape(groups_ep, local_experts, capacity, local_width)
    answers = run_experts(
        lax.all_to_all(outgoing, "ep", split_axis=0, concat_axis=0, tiled=True),
        w_gate,
        w_up,
        w_down,
    )
    returned = lax.all_to_all(answers, "ep", split_axis=0, concat_axis=0, tiled=True)
    flat_out = returned.reshape(experts * capacity, local_width)
    picked = flat_out[position].reshape(tok_rows, top_count, local_width)
    combined = jnp.sum(my_weights[:, :, None] * picked.astype(jnp.float32), axis=1)
    out_squares = lax.psum(jnp.sum(combined * combined, axis=1), "tp")
    return (combined * lax.rsqrt(out_squares / D + EPS)[:, None] * out_gain).astype(jnp.bfloat16)


def solution(mesh):
    placed = (
        P("ep", "tp"),
        P("tp"),
        P("tp"),
        P(),
        P(),
        P("ep", "tp", None),
        P("ep", "tp", None),
        P("ep", None, "tp"),
    )
    return jax.shard_map(
        on_device, mesh=mesh, in_specs=placed, out_specs=P("ep", "tp"), check_vma=False
    )
```

profile of v0, /device:TPU:0, one launch (start us, length us, event | category | flops | bytes accessed | tf_op | source)
XLA Modules:
  0.0 185.9 jit_solution(116999732136430107)
XLA Ops:
  6.5 0.0 copy-start
  6.5 0.0 all-reduce.3.cloned.1.call-start
  6.5 0.7 copy-done
  7.2 0.1 constant_dynamic-slice_fusion
  7.3 0.1 copy.33
  7.4 0.1 eq.42
  7.5 0.1 eq.38
  7.6 0.6 reduce-window.6
  8.2 0.2 slice_reduce_fusion
  8.5 0.1 fusion.42
  8.6 0.1 reduce_sum.41
  8.7 0.1 copy.26
  8.8 0.1 fusion.33
  8.9 1.0 fusion.34
  10.0 11.4 %psum.28 = f32[64]{0:T(128)S(1)} all-reduce(f32[64]{0:T(128)S(1)} %fusion.34), channel_id=1, replica_groups=mesh['ep'=8,'tp'=4] {'tp'}, use_global_device_ids=true, to_apply=%region_5.6 | all-reduce | flops 64 | bytes 512 | tf_op jit(solution)/shard_map/psum | solution.py:35
  21.4 1.4 convolution_convert_fusion
  22.8 31.2 %all_to_all.10 = bf16[8,4,16,1024]{3,2,1,0:T(8,128)(2,1)S(1)} all-to-all(bf16[8,4,16,1024]{3,2,1,0:T(8,128)(2,1)S(1)} %bitcast.58), channel_id=1, replica_groups=mesh['ep'=8,'tp'=4] {'ep'}, dimensions={0} | all-to-all | bytes 2097152 | tf_op jit(solution)/shard_map/all_to_all | solution.py:54
  54.0 0.0 copy-start.1
  54.0 5.9 %fusion.23 = bf16[8,4,16,1024]{3,2,0,1:T(8,128)(2,1)} fusion(bf16[4,1024,1024]{2,1,0:T(8,128)(2,1)} %param.14, bf16[8,4,16,1024]{3,2,1,0:T(8,128)(2,1)S(1)} %all_to_all.10), kind=kOutput, calls=%fused_computation.19 | convolution fusion | flops 1074266112 | bytes 10485760 | tf_op jit(solution)/shard_map/secd,edf->secf/dot_general | solution.py:14
  59.9 0.0 copy-done.1
  59.9 2.3 %fusion.26 = bf16[8,4,16,1024]{3,2,0,1:T(8,128)(2,1)} fusion(bf16[4,1024,1024]{2,1,0:T(8,128)(2,1)S(1)} %copy-done.1, bf16[8,4,16,1024]{3,2,1,0:T(8,128)(2,1)S(1)} %all_to_all.10), kind=kOutput, calls=%fused_computation.20 | convolution fusion | flops 1074266112 | bytes 10485760 | tf_op jit(solution)/shard_map/secd,edf->secf/dot_general | solution.py:11
  62.1 0.0 all-reduce.3.cloned.1.call-update
  62.2 66.7 %all-reduce.3.cloned.1.call-done = (bf16[8,4,16,1024]{3,2,0,1:T(8,128)(2,1)}, bf16[8,4,16,1024]{3,2,0,1:T(8,128)(2,1)}) async-done(((bf16[8,4,16,1024]{3,2,0,1:T(8,128)(2,1)}, bf16[8,4,16,1024]{3,2,0,1:T(8,128)(2,1)}), (bf16[8,4,16,1024]{3,2,0,1:T(8,128)(2,1)}, bf16[8,4,16,1024]{3,2,0,1:T(8,128)(2,1)})) %all-reduce.3.cloned.1.call-update) | async-done | bytes 2097168 | tf_op jit(solution)/shard_map/psum | solution.py:19
  128.9 5.9 %fusion.20 = bf16[8,4,16,1024]{3,2,0,1:T(8,128)(2,1)S(1)} fusion(bf16[4,1024,1024]{2,1,0:T(8,128)(2,1)} %param.15, bf16[8,4,16,1024]{3,2,0,1:T(8,128)(2,1)} %get-tuple-element.5, bf16[8,4,16,1024]{3,2,0,1:T(8,128)(2,1)} %get-tuple-element.6), kind=kOutput, calls=%fused_computation.18 | convolution fusion | flops 1078460416 | bytes 11534336 | tf_op jit(solution)/shard_map/secf,efd->secd/dot_general | solution.py:22
  134.8 1.1 copy.29
  135.9 4.6 %all-to-all-start.1 = ((bf16[8,4,16,1024]{3,2,1,0:T(8,128)(2,1)}), bf16[8,4,16,1024]{3,2,1,0:T(8,128)(2,1)S(1)}, u32[]{:S(2)}, u32[]{:S(2)}) async-start(bf16[8,4,16,1024]{3,2,1,0:T(8,128)(2,1)} %copy.29), calls=%async_computation.1 | async-start | bytes 2097152 | tf_op jit(solution)/shard_map/all_to_all | solution.py:59
  140.5 0.1 mul.89
  140.6 0.8 constant_dynamic-slice_fusion.1
  141.3 0.1 copy.23
  141.5 25.6 %all-to-all-done.1 = bf16[8,4,16,1024]{3,2,1,0:T(8,128)(2,1)S(1)} async-done(((bf16[8,4,16,1024]{3,2,1,0:T(8,128)(2,1)}), bf16[8,4,16,1024]{3,2,1,0:T(8,128)(2,1)S(1)}, u32[]{:S(2)}, u32[]{:S(2)}) %all-to-all-start.1) | async-done | bytes 1048608 | tf_op jit(solution)/shard_map/all_to_all | solution.py:59
  167.0 1.2 gather_fusion
  168.2 0.0 copy-start.2
  168.2 0.3 reshape.70
  168.6 0.7 multiply_reduce_fusion
  169.3 0.1 multiply_reduce_fusion.1
  169.4 8.9 %psum.31 = f32[64]{0:T(128)S(1)} all-reduce(f32[64]{0:T(128)S(1)} %multiply_reduce_fusion.1), channel_id=1, replica_groups=mesh['ep'=8,'tp'=4] {'tp'}, use_global_device_ids=true, to_apply=%region_10.11 | all-reduce | flops 64 | bytes 512 | tf_op jit(solution)/shard_map/psum | solution.py:63
  178.3 0.0 copy-done.2
  178.3 0.8 multiply_convert_fusion
  (8 shorter events, 0.1 us)
Async XLA Ops:
  6.5 0.7 copy-start
  6.5 122.3 %all-reduce.3.cloned.1.call-start = ((), (), s32[]{:S(2)}) async-start(), calls=%async_computation.2 | async-start | bytes 4194304 | tf_op jit(solution)/shard_map/psum | solution.py:19
  54.0 5.9 %copy-start.1 = (bf16[4,1024,1024]{2,1,0:T(8,128)(2,1)S(1)}, bf16[4,1024,1024]{2,1,0:T(8,128)(2,1)}, u32[]{:S(2)}) copy-start(bf16[4,1024,1024]{2,1,0:T(8,128)(2,1)} %param.13) | copy-start | bytes 25165828
  135.9 31.2 %all-to-all-start.1 = ((bf16[8,4,16,1024]{3,2,1,0:T(8,128)(2,1)}), bf16[8,4,16,1024]{3,2,1,0:T(8,128)(2,1)S(1)}, u32[]{:S(2)}, u32[]{:S(2)}) async-start(bf16[8,4,16,1024]{3,2,1,0:T(8,128)(2,1)} %copy.29), calls=%async_computation.1 | async-start | bytes 2097152 | tf_op jit(solution)/shard_map/all_to_all | solution.py:59
  168.2 10.1 %copy-start.2 = (f32[1024]{0:T(1024)S(1)}, f32[1024]{0:T(1024)}, u32[]{:S(2)}) copy-start(f32[1024]{0:T(1024)} %param.10) | copy-start | bytes 12292
Sparse Core Ops, SparseCore 0:
  62.3 66.5 all-reduce.2
where the time goes:
time: 186 us
  waiting for transfers between devices  92.3 us (50%)
  blocking collectives  51.6 us (28%)
  matrix products  15.4 us (8%)
  between operations  13.5 us (7%)
  local copies, waits for them, and re-layouts  5.01 us (3%)
  starting transfers between devices  4.61 us (2%)
  other arithmetic  3.53 us (2%)
    psum x1, waiting for transfers between devices, run_experts(): lax.psum(up_part, 'tp').astype(jnp.float32)  66.7 us
    all_to_all x1, blocking collectives, on_device(): lax.all_to_all(outgoing, 'ep', split_axis=0, concat_axis=0, tiled=True)  31.2 us
    all_to_all x1, waiting for transfers between devices, on_device(): lax.all_to_all(answers, 'ep', split_axis=0, concat_axis=0, tiled=True)  25.6 us
    psum x1, blocking collectives, on_device(): sum_squares = lax.psum(jnp.sum(values * values, axis=1), 'tp')  11.4 us
    psum x1, blocking collectives, on_device(): out_squares = lax.psum(jnp.sum(combined * combined, axis=1), 'tp')  8.93 us
    dot_general x1, matrix products, run_experts(): jnp.einsum('secf,efd->secd', active, w_down, preferred_element_type=jnp.f...  5.89 us
    dot_general x1, matrix products, run_experts(): jnp.einsum('secd,edf->secf', slot_rows, w_up, preferred_element_type=jnp....  5.86 us
    all_to_all x1, starting transfers between devices, on_device(): lax.all_to_all(answers, 'ep', split_axis=0, concat_axis=0, tiled=True)  4.61 us
  transfers between devices with their start and end apart: 2, of which 2 were waited for; matrix products, arithmetic and copies ran while one was open for 1% of the time, Pallas kernels for 0%

commit v1 on v0

--- a/solution.py
+++ b/solution.py
@@ -32,7 +32,7 @@
     experts = local_experts * groups_ep
     capacity = max(2, 2 * tok_rows * top_count // experts)
     values = tokens.astype(jnp.float32)
-    sum_squares = lax.psum(jnp.sum(values * values, axis=1), "tp")
+    sum_squares = jnp.sum(lax.all_gather(jnp.sum(values * values, axis=1), axis_name="tp"), 0)
     normed = (values * lax.rsqrt(sum_squares / D + EPS)[:, None] * in_gain).astype(jnp.bfloat16)
     row_start = lax.axis_index("ep") * tok_rows
     my_routes = lax.dynamic_slice_in_dim(routes, row_start, tok_rows, 0)

time: 186 us -> 189 us (1.016)
    psum x1 -> x0, blocking collectives: 11.4 us -> none  [on_device(): sum_squares = lax.psum(jnp.sum(values * values, axis=1), 'tp')]
    unnamed x0 -> x1, blocking collectives: none -> 11.4 us
where the time goes in v1:
time: 189 us; the launch traced here: 188 us
  waiting for transfers between devices  92.3 us (49%)
  blocking collectives  51.5 us (27%)
  matrix products  15.5 us (8%)
  between operations  14.2 us (8%)
  local copies, waits for them, and re-layouts  6.59 us (3%)
  starting transfers between devices  4.61 us (2%)
  other arithmetic  3.55 us (2%)
    psum x1, waiting for transfers between devices, run_experts(): lax.psum(up_part, 'tp').astype(jnp.float32)  66.7 us
    all_to_all x1, blocking collectives, on_device(): lax.all_to_all(outgoing, 'ep', split_axis=0, concat_axis=0, tiled=True)  31.2 us
    all_to_all x1, waiting for transfers between devices, on_device(): lax.all_to_all(answers, 'ep', split_axis=0, concat_axis=0, tiled=True)  25.6 us
    unnamed x1, blocking collectives  11.4 us
    psum x1, blocking collectives, on_device(): out_squares = lax.psum(jnp.sum(combined * combined, axis=1), 'tp')  8.93 us
    dot_general x1, matrix products, run_experts(): jnp.einsum('secf,efd->secd', active, w_down, preferred_element_type=jnp.f...  5.9 us
    dot_general x1, matrix products, run_experts(): jnp.einsum('secd,edf->secf', slot_rows, w_up, preferred_element_type=jnp....  5.87 us
    all_to_all x1, starting transfers between devices, on_device(): lax.all_to_all(answers, 'ep', split_axis=0, concat_axis=0, tiled=True)  4.6 us
  transfers between devices with their start and end apart: 2, of which 2 were waited for; matrix products, arithmetic and copies ran while one was open for 1% of the time, Pallas kernels for 0%

profile of v1, /device:TPU:0, one launch (start us, length us, event | category | flops | bytes accessed | tf_op | source)
XLA Modules:
  0.0 188.2 jit_solution(4468226945776824936)
XLA Ops:
  6.5 0.0 copy-start
  6.5 0.0 all-reduce.4.cloned.1.call-start
  6.5 0.7 copy-done
  7.2 0.1 constant_dynamic-slice_fusion
  7.3 0.1 copy.33
  7.4 0.1 eq.42
  7.5 0.1 eq.38
  7.6 0.6 reduce-window.6
  8.2 0.2 slice_reduce_fusion
  8.5 0.1 fusion.42
  8.6 0.1 reduce_sum.50
  8.7 0.1 copy.26
  8.8 0.1 fusion.33
  8.9 1.0 fusion.34
  10.0 1.2 dynamic-slice
  11.9 0.2 dynamic-update-slice
  12.1 11.4 %all-reduce = f32[256]{0:T(256)S(1)} all-reduce(f32[256]{0:T(256)S(1)} %dynamic-update-slice), channel_id=2, replica_groups=mesh['ep'=8,'tp'=4] {'tp'}, use_global_device_ids=true, to_apply=%add | all-reduce | flops 256 | bytes 2048
  23.5 0.1 reshape.83
  23.6 1.4 convolution_convert_fusion
  25.0 31.2 %all_to_all.10 = bf16[8,4,16,1024]{3,2,1,0:T(8,128)(2,1)S(1)} all-to-all(bf16[8,4,16,1024]{3,2,1,0:T(8,128)(2,1)S(1)} %bitcast.59), channel_id=1, replica_groups=mesh['ep'=8,'tp'=4] {'ep'}, dimensions={0} | all-to-all | bytes 2097152 | tf_op jit(solution)/shard_map/all_to_all | solution.py:54
  56.3 0.0 copy-start.1
  56.3 5.9 %fusion.23 = bf16[8,4,16,1024]{3,2,0,1:T(8,128)(2,1)} fusion(bf16[4,1024,1024]{2,1,0:T(8,128)(2,1)} %param.14, bf16[8,4,16,1024]{3,2,1,0:T(8,128)(2,1)S(1)} %all_to_all.10), kind=kOutput, calls=%fused_computation.19 | convolution fusion | flops 1074266112 | bytes 10485760 | tf_op jit(solution)/shard_map/secd,edf->secf/dot_general | solution.py:14
  62.1 0.0 copy-done.1
  62.1 2.3 %fusion.26 = bf16[8,4,16,1024]{3,2,0,1:T(8,128)(2,1)} fusion(bf16[4,1024,1024]{2,1,0:T(8,128)(2,1)S(1)} %copy-done.1, bf16[8,4,16,1024]{3,2,1,0:T(8,128)(2,1)S(1)} %all_to_all.10), kind=kOutput, calls=%fused_computation.20 | convolution fusion | flops 1074266112 | bytes 10485760 | tf_op jit(solution)/shard_map/secd,edf->secf/dot_general | solution.py:11
  64.4 0.0 all-reduce.4.cloned.1.call-update
  64.4 66.7 %all-reduce.4.cloned.1.call-done = (bf16[8,4,16,1024]{3,2,0,1:T(8,128)(2,1)}, bf16[8,4,16,1024]{3,2,0,1:T(8,128)(2,1)}) async-done(((bf16[8,4,16,1024]{3,2,0,1:T(8,128)(2,1)}, bf16[8,4,16,1024]{3,2,0,1:T(8,128)(2,1)}), (bf16[8,4,16,1024]{3,2,0,1:T(8,128)(2,1)}, bf16[8,4,16,1024]{3,2,0,1:T(8,128)(2,1)})) %all-reduce.4.cloned.1.call-update) | async-done | bytes 2097168 | tf_op jit(solution)/shard_map/psum | solution.py:19
  131.1 5.9 %fusion.20 = bf16[8,4,16,1024]{3,2,0,1:T(8,128)(2,1)S(1)} fusion(bf16[4,1024,1024]{2,1,0:T(8,128)(2,1)} %param.15, bf16[8,4,16,1024]{3,2,0,1:T(8,128)(2,1)} %get-tuple-element.5, bf16[8,4,16,1024]{3,2,0,1:T(8,128)(2,1)} %get-tuple-element.6), kind=kOutput, calls=%fused_computation.18 | convolution fusion | flops 1078460416 | bytes 11534336 | tf_op jit(solution)/shard_map/secf,efd->secd/dot_general | solution.py:22
  137.0 1.1 copy.29
  138.1 4.6 %all-to-all-start.1 = ((bf16[8,4,16,1024]{3,2,1,0:T(8,128)(2,1)}), bf16[8,4,16,1024]{3,2,1,0:T(8,128)(2,1)S(1)}, u32[]{:S(2)}, u32[]{:S(2)}) async-start(bf16[8,4,16,1024]{3,2,1,0:T(8,128)(2,1)} %copy.29), calls=%async_computation.1 | async-start | bytes 2097152 | tf_op jit(solution)/shard_map/all_to_all | solution.py:59
  142.7 0.1 mul.89
  142.8 0.8 constant_dynamic-slice_fusion.1
  143.6 0.1 copy.23
  143.7 25.6 %all-to-all-done.1 = bf16[8,4,16,1024]{3,2,1,0:T(8,128)(2,1)S(1)} async-done(((bf16[8,4,16,1024]{3,2,1,0:T(8,128)(2,1)}), bf16[8,4,16,1024]{3,2,1,0:T(8,128)(2,1)S(1)}, u32[]{:S(2)}, u32[]{:S(2)}) %all-to-all-start.1) | async-done | bytes 1048608 | tf_op jit(solution)/shard_map/all_to_all | solution.py:59
  169.3 1.2 gather_fusion
  170.5 0.0 copy-start.2
  170.5 0.3 reshape.74
  170.8 0.7 multiply_reduce_fusion
  171.5 0.1 multiply_reduce_fusion.1
  171.6 8.9 %psum.23 = f32[64]{0:T(128)S(1)} all-reduce(f32[64]{0:T(128)S(1)} %multiply_reduce_fusion.1), channel_id=1, replica_groups=mesh['ep'=8,'tp'=4] {'tp'}, use_global_device_ids=true, to_apply=%region_10.11 | all-reduce | flops 64 | bytes 512 | tf_op jit(solution)/shard_map/psum | solution.py:63
  180.6 0.0 copy-done.2
  180.6 0.8 multiply_convert_fusion
  (10 shorter events, 0.1 us)
Async XLA Ops:
  6.5 0.7 copy-start
  6.5 124.6 %all-reduce.4.cloned.1.call-start = ((), (), s32[]{:S(2)}) async-start(), calls=%async_computation.2 | async-start | bytes 4194304 | tf_op jit(solution)/shard_map/psum | solution.py:19
  56.3 5.9 %copy-start.1 = (bf16[4,1024,1024]{2,1,0:T(8,128)(2,1)S(1)}, bf16[4,1024,1024]{2,1,0:T(8,128)(2,1)}, u32[]{:S(2)}) copy-start(bf16[4,1024,1024]{2,1,0:T(8,128)(2,1)} %param.13) | copy-start | bytes 25165828
  138.1 31.2 %all-to-all-start.1 = ((bf16[8,4,16,1024]{3,2,1,0:T(8,128)(2,1)}), bf16[8,4,16,1024]{3,2,1,0:T(8,128)(2,1)S(1)}, u32[]{:S(2)}, u32[]{:S(2)}) async-start(bf16[8,4,16,1024]{3,2,1,0:T(8,128)(2,1)} %copy.29), calls=%async_computation.1 | async-start | bytes 2097152 | tf_op jit(solution)/shard_map/all_to_all | solution.py:59
  170.5 10.1 %copy-start.2 = (f32[1024]{0:T(1024)S(1)}, f32[1024]{0:T(1024)}, u32[]{:S(2)}) copy-start(f32[1024]{0:T(1024)} %param.10) | copy-start | bytes 12292
Sparse Core Ops, SparseCore 0:
  64.5 66.5 all-reduce.3
